TPU v7x, 32 devices: a whole 2x2x4 slice. The times are simulated.
32 devices in a mesh: ra: 4 (over z), cb: 4 (over y, x), dp: 2 (over core).
Axes of the slice: x: 2, y: 2, z: 4, core: 2. Of those that a mesh axis runs over, the one named last changes fastest.
Arguments:
- carried: bfloat16 [3072, 4096], P('dp', 'ra'), may hold values from -100 to 100
- branch_in: bfloat16 [3072, 4096], P('dp', 'ra'), may hold values from -12 to 12
- gain_in: float32 [4096], P('ra'), may hold values from 0.1 to 1.9
- bias_in: float32 [4096], P('ra'), may hold values from -1.8 to 1.8
- up_weight: bfloat16 [4096, 16384], P('ra', 'cb'), may hold values from -0.125 to 0.125
- down_weight: bfloat16 [16384, 4096], P('cb', 'ra'), may hold values from -0.046875 to 0.046875
- gain_out: float32 [4096], P('ra'), may hold values from 0.1 to 1.9
- bias_out: float32 [4096], P('ra'), may hold values from -1.8 to 1.8
Outputs:
- layer_out: bfloat16 [3072, 4096], P('dp', 'ra')
All inputs are finite; a program needn't handle non-finite values.
Results may differ from a plain program's by a relative error of at most 0.006.
Values may be sent and summed in bfloat16 or wider, within the bound.
A program may use at most 128 MiB of HBM per device.

v0:
```python
import jax
import jax.numpy as jnp
from jax import lax
from jax.sharding import PartitionSpec as P

residual_scale = 2.0**0.25
norm_eps = 1e-05


def normalize(mixed, totals, squares, width, gain, bias):
    mean = totals[:, None] / width
    spread = squares[:, None] / width - mean * mean
    return (mixed - mean) * lax.rsqrt(spread + norm_eps) * gain + bias


def per_device(carried, branch_in, gain_in, bias_in, up_weight, down_weight, gain_out, bias_out):
    width = carried.shape[1] * lax.axis_size("ra")
    mixed_in = residual_scale * carried.astype(jnp.float32) + branch_in.astype(jnp.float32)
    totals, squares = lax.psum(
        (jnp.sum(mixed_in, axis=1), jnp.sum(mixed_in * mixed_in, axis=1)), "ra"
    )
    normed = normalize(mixed_in, totals, squares, width, gain_in, bias_in).astype(jnp.bfloat16)
    regrouped = lax.all_to_all(up_weight, "ra", split_axis=1, concat_axis=0, tiled=True)
    pre_share = lax.dot_general(
        regrouped,
        lax.all_gather(normed, "ra", axis=1, tiled=True),
        (((0,), (1,)), ((), ())),
        preferred_element_type=jnp.float32,
    )
    hidden_share = jnp.square(jnp.maximum(pre_share, 0.0)).astype(jnp.bfloat16)
    branch_part = lax.dot_general(
        lax.all_gather(hidden_share, "ra", axis=0, tiled=True),
        down_weight,
        (((0,), (0,)), ((), ())),
        preferred_element_type=jnp.float32,
    )
    branch_out = lax.psum(branch_part, "cb")
    mixed_out = residual_scale * normed.astype(jnp.float32) + branch_out
    totals_out, squares_out = lax.psum(
        (jnp.sum(mixed_out, axis=1), jnp.sum(mixed_out * mixed_out, axis=1)), "ra"
    )
    return normalize(mixed_out, totals_out, squares_out, width, gain_out, bias_out).astype(
        jnp.bfloat16
    )


def solution(mesh):
    in_specs = (
        P("dp", "ra"),
        P("dp", "ra"),
        P("ra"),
        P("ra"),
        P("ra", "cb"),
        P("cb", "ra"),
        P("ra"),
        P("ra"),
    )
    out_specs = P("dp", "ra")
    return jax.shard_map(
        per_device, mesh=mesh, in_specs=in_specs, out_specs=out_specs, check_vma=False
    )
```

profile of v0, /device:TPU:0, one launch (start us, length us, event | category | flops | bytes accessed | tf_op | source)
XLA Modules:
  0.0 859.6 jit_solution(17207012379904280185)
XLA Ops:
  6.5 0.0 copy-start.1
  6.5 0.0 copy-start.2
  6.5 0.0 copy-start.3
  6.5 0.0 all-gather.3.cloned.1.call-start
  6.5 4.5 fusion
  11.1 20.5 %all-reduce.1 = (f32[1536]{0:T(1024)S(1)}, f32[1536]{0:T(1024)S(1)}) all-reduce(f32[1536]{0:T(1024)S(1)} %get-tuple-element.8, f32[1536]{0:T(1024)S(1)} %get-tuple-element.7), channel_id=1, replica_groups=mesh['ra'=4,'cb'=4,'dp'=2] {'ra'}, use_global_device_ids=true, to_apply=%region_3.0 | all-reduce | flops 3072 | bytes 24576 | tf_op jit(solution)/shard_map/psum | solution.py:19
  31.6 0.0 copy-done.1
  31.6 0.0 copy-done.2
  31.6 0.0 copy-done.3
  31.6 4.5 add_convert_fusion.1
  36.2 0.0 all-gather.3.cloned.1.call-update
  36.2 0.0 all-gather.5.cloned.1.call-start
  36.2 12.2 %copy.9 = bf16[1024,4096]{0,1:T(8,128)(2,1)} copy(bf16[1024,4096]{1,0:T(8,128)(2,1)} %param.12) | data formatting | bytes 16777216 | tf_op args[4]
  48.5 373.1 %all_to_all.19 = bf16[1024,4,1024]{0,2,1:T(8,128)(2,1)} all-to-all(bf16[1024,4,1024]{0,2,1:T(8,128)(2,1)} %bitcast.10), channel_id=1, replica_groups=mesh['ra'=4,'cb'=4,'dp'=2] {'ra'}, dimensions={1} | all-to-all | bytes 16777216 | tf_op jit(solution)/shard_map/all_to_all | solution.py:23
  421.6 11.4 %copy.10 = bf16[4,1024,1024]{2,1,0:T(8,128)(2,1)} copy(bf16[4,1024,1024]{1,2,0:T(8,128)(2,1)} %bitcast.9) | data formatting | bytes 16777216 | tf_op jit(solution)/shard_map/all_to_all | solution.py:23
  432.9 0.0 all-gather.3.cloned.1.call-done
  432.9 19.2 %fusion.1 = bf16[1024,1536]{0,1:T(8,128)(2,1)} fusion(bf16[1536,4096]{1,0:T(8,128)(2,1)} %all-gather.3.cloned.1.call-done, bf16[4096,1024]{1,0:T(8,128)(2,1)} %bitcast.11), kind=kOutput, calls=%fused_computation.8 | convolution fusion | flops 12889620480 | bytes 24117248 | tf_op jit(solution)/shard_map/dot_general | solution.py:24
  452.1 0.0 all-gather.5.cloned.1.call-update
  452.1 0.2 all-reduce.4.cloned.1.call-start
  452.3 216.9 %all-gather.5.cloned.1.call-done = bf16[4096,1536]{0,1:T(8,128)(2,1)} async-done(((bf16[1024,1536]{0,1:T(8,128)(2,1)}), bf16[4096,1536]{0,1:T(8,128)(2,1)}) %all-gather.5.cloned.1.call-update) | async-done | bytes 12582928 | tf_op jit(solution)/shard_map/all_gather | solution.py:32
  669.2 19.5 %fusion.3 = f32[1536,1024]{1,0:T(8,128)} fusion(bf16[4096,1536]{0,1:T(8,128)(2,1)} %all-gather.5.cloned.1.call-done, bf16[4096,1024]{1,0:T(8,128)(2,1)} %param.13), kind=kOutput, calls=%fused_computation.14 | convolution fusion | flops 12884901888 | bytes 27262976 | tf_op jit(solution)/shard_map/dot_general | solution.py:31
  688.7 0.0 copy-start
  688.7 0.0 all-reduce.4.cloned.1.call-update
  688.8 0.0 copy-start.4
  688.8 0.0 copy-start.5
  688.8 136.5 %all-reduce.4.cloned.1.call-done = f32[1536,1024]{1,0:T(8,128)} async-done(((f32[1536,1024]{1,0:T(8,128)}), f32[1536,1024]{1,0:T(8,128)}) %all-reduce.4.cloned.1.call-update) | async-done | bytes 6291472 | tf_op jit(solution)/shard_map/psum | solution.py:37
  825.3 0.0 copy-done
  825.3 4.1 fusion.2
  829.4 18.7 %all-reduce = (f32[1536]{0:T(1024)S(1)}, f32[1536]{0:T(1024)S(1)}) all-reduce(f32[1536]{0:T(1024)S(1)} %get-tuple-element.6, f32[1536]{0:T(1024)S(1)} %get-tuple-element.5), channel_id=1, replica_groups=mesh['ra'=4,'cb'=4,'dp'=2] {'ra'}, use_global_device_ids=true, to_apply=%region_8.0 | all-reduce | flops 3072 | bytes 24576 | tf_op jit(solution)/shard_map/psum | solution.py:39
  848.1 0.0 copy-done.4
  848.1 0.0 copy-done.5
  848.1 4.9 add_convert_fusion
  (2 shorter events, 0.0 us)
Async XLA Ops:
  6.5 25.1 %copy-start.1 = (bf16[1536,1024]{1,0:T(8,128)(2,1)S(1)}, bf16[1536,1024]{1,0:T(8,128)(2,1)}, u32[]{:S(2)}) copy-start(bf16[1536,1024]{1,0:T(8,128)(2,1)} %param.9) | copy-start | bytes 9437188
  6.5 25.1 %copy-start.2 = (f32[1024]{0:T(1024)S(1)}, f32[1024]{0:T(1024)}, u32[]{:S(2)}) copy-start(f32[1024]{0:T(1024)} %param.11) | copy-start | bytes 12292
  6.5 25.1 %copy-start.3 = (f32[1024]{0:T(1024)S(1)}, f32[1024]{0:T(1024)}, u32[]{:S(2)}) copy-start(f32[1024]{0:T(1024)} %param.10) | copy-start | bytes 12292
  6.5 426.4 %all-gather.3.cloned.1.call-start = ((), (), s32[]{:S(2)}) async-start(), calls=%async_computation.1 | async-start | bytes 15728640 | tf_op jit(solution)/shard_map/all_gather | solution.py:26
  36.2 633.1 %all-gather.5.cloned.1.call-start = ((), (), s32[]{:S(2)}) async-start(), calls=%async_computation.2 | async-start | bytes 15728640 | tf_op jit(solution)/shard_map/all_gather | solution.py:32
  452.1 373.1 %all-reduce.4.cloned.1.call-start = ((), (), s32[]{:S(2)}) async-start(), calls=%async_computation.3 | async-start | bytes 12582912 | tf_op jit(solution)/shard_map/psum | solution.py:37
  688.7 136.5 %copy-start = (bf16[1536,1024]{1,0:T(8,128)(2,1)S(1)}, bf16[1536,1024]{1,0:T(8,128)(2,1)}, u32[]{:S(2)}) copy-start(bf16[1536,1024]{1,0:T(8,128)(2,1)} %add_convert_fusion.1) | copy-start | bytes 9437188
  688.8 159.4 %copy-start.4 = (f32[1024]{0:T(1024)S(1)}, f32[1024]{0:T(1024)}, u32[]{:S(2)}) copy-start(f32[1024]{0:T(1024)} %param.15) | copy-start | bytes 12292
  688.8 159.4 %copy-start.5 = (f32[1024]{0:T(1024)S(1)}, f32[1024]{0:T(1024)}, u32[]{:S(2)}) copy-start(f32[1024]{0:T(1024)} %param.14) | copy-start | bytes 12292
Sparse Core Ops, SparseCore 0:
  36.3 395.6 all-gather.2
  452.2 216.9 all-gather.4
  688.9 136.3 all-reduce.3
where the time goes:
time: 860 us
  blocking collectives  412 us (48%)
  waiting for transfers between devices  353 us (41%)
  matrix products  38.6 us (4%)
  local copies, waits for them, and re-layouts  23.6 us (3%)
  other arithmetic  18.1 us (2%)
  between operations  13.2 us (2%)
    all_to_all x1, blocking collectives, per_device(): lax.all_to_all(up_weight, 'ra', split_axis=1, concat_axis=0, tiled=True)  373 us
    all_gather x1, waiting for transfers between devices, per_device(): lax.all_gather(hidden_share, 'ra', axis=0, tiled=True)  217 us
    psum x1, waiting for transfers between devices, per_device(): branch_out = lax.psum(branch_part, 'cb')  136 us
    psum x1, blocking collectives, per_device(): lax.psum((jnp.sum(mixed_in, axis=1), jnp.sum(mixed_in * mixed_in, axis=1)...  20.5 us
    dot_general x1, matrix products, per_device(): lax.dot_general(lax.all_gather(hidden_share, 'ra', axis=0, tiled=True), d...  19.5 us
    dot_general x1, matrix products, per_device(): lax.dot_general(regrouped, lax.all_gather(normed, 'ra', axis=1, tiled=Tru...  19.2 us
    psum x1, blocking collectives, per_device(): lax.psum((jnp.sum(mixed_out, axis=1), jnp.sum(mixed_out * mixed_out, axis...  18.7 us
  transfers between devices with their start and end apart: 3, of which 2 were waited for; matrix products, arithmetic and copies ran while one was open for 3% of the time, Pallas kernels for 0%

commit v1 on v0

v1 whole, which is shorter than its diff:
```python
import functools
import math

import jax
import jax.numpy as jnp
from jax import lax
from jax.experimental import pallas as pl
from jax.experimental.pallas import tpu as pltpu
from jax.sharding import PartitionSpec as P

residual_scale = 2.0**0.25
norm_eps = 1e-05
lookahead = 2


def kernel(n, m, nd, block, x_hbm, w1_hbm, w2_hbm, gain_ref, bias_ref, o_hbm,
           xall, w1s, h, w2, part, rs_src, rs_recv, mixed, st_src, st_recv, fin,
           loc_sem, w1_send, w1_recv, dp_send, dp_recv, xz_r, xz_l, xz_recv,
           xy_send, xy_recv, h_r, h_l, h_recv, rs_send, rs_rcv, st_send, st_rcv,
           fin_send, fin_rcv):
    me, cb, dp = lax.axis_index("ra"), lax.axis_index("cb"), lax.axis_index("dp")
    _, tokens, dl = xall.shape
    fs = w1s.shape[2]
    blocks = tokens // block
    quarter = tokens // m
    rows = block // m
    half = dl // nd
    width = n * dl
    tile = math.gcd(256, math.gcd(fs, dl))

    barrier = pltpu.get_barrier_semaphore()
    for o in range(1, n):
        pl.semaphore_signal(barrier, inc=1, device_id={"ra": lax.rem(me + o, n)})
    for o in range(1, m):
        pl.semaphore_signal(barrier, inc=1, device_id={"cb": lax.rem(cb + o, m)})
    for o in range(1, nd):
        pl.semaphore_signal(barrier, inc=1, device_id={"dp": lax.rem(dp + o, nd)})

    own_x = pltpu.make_async_copy(x_hbm, xall.at[me], loc_sem.at[0])
    own_w1 = pltpu.make_async_copy(
        w1_hbm.at[:, pl.ds(pl.multiple_of(me * fs, fs), fs)], w1s.at[me], loc_sem.at[1])
    own_w2 = pltpu.make_async_copy(w2_hbm, w2, loc_sem.at[2])
    own_x.start()
    own_w1.start()
    own_w2.start()
    pl.semaphore_wait(barrier, n + m + nd - 3)
    own_x.wait()

    def at_rows(start, size):
        return pl.ds(pl.multiple_of(start, size), size)

    def line(ref_of, right_sem, left_sem, recv_sem, src, to_right):
        ref = ref_of(src)
        return pltpu.make_async_remote_copy(
            src_ref=ref, dst_ref=ref,
            send_sem=(right_sem if to_right else left_sem)(src),
            recv_sem=recv_sem(src),
            device_id={"ra": jnp.minimum(me + 1, n - 1) if to_right else jnp.maximum(me - 1, 0)})

    def start_own(make):
        @pl.when(me + 1 < n)
        def _():
            make(me, True).start()

        @pl.when(me >= 1)
        def _():
            make(me, False).start()

    def relay(make, landed):
        for s in range(1, n):
            @pl.when(me - s >= 0)
            def _():
                make(me - s, True).wait_recv()

                @pl.when(me + 1 < n)
                def _():
                    make(me - s, True).start()
                landed(me - s)

            @pl.when(me + s < n)
            def _():
                make(me + s, False).wait_recv()

                @pl.when(me >= 1)
                def _():
                    make(me + s, False).start()
                landed(me + s)

    def line_sent(make):
        for s in range(n):
            @pl.when((me - s >= 0) & (me + 1 < n))
            def _():
                make(me - s, True).wait_send()

            @pl.when((me + s < n) & (me >= 1))
            def _():
                make(me + s, False).wait_send()

    make_x = functools.partial(
        line, lambda s: xall.at[s, at_rows(cb * quarter, quarter)],
        lambda s: xz_r.at[s], lambda s: xz_l.at[s], lambda s: xz_recv.at[s])

    def xy_copy(src, o):
        ref = xall.at[src, at_rows(cb * quarter, quarter)]
        return pltpu.make_async_remote_copy(
            src_ref=ref, dst_ref=ref, send_sem=xy_send.at[src, o], recv_sem=xy_recv.at[src, cb],
            device_id={"cb": lax.rem(cb + o, m)})

    def xy_landed(src, o):
        sender = lax.rem(cb + o, m)
        ref = xall.at[src, at_rows(sender * quarter, quarter)]
        return pltpu.make_async_remote_copy(
            src_ref=ref, dst_ref=ref, send_sem=xy_send.at[src, o], recv_sem=xy_recv.at[src, sender],
            device_id={"cb": sender})

    def w1_copy(o):
        to = lax.rem(me + o, n)
        return pltpu.make_async_remote_copy(
            src_ref=w1_hbm.at[at_rows(dp * half, half), pl.ds(pl.multiple_of(to * fs, fs), fs)],
            dst_ref=w1s.at[me, at_rows(dp * half, half)],
            send_sem=w1_send.at[to], recv_sem=w1_recv.at[me], device_id={"ra": to})

    def w1_landed(o):
        src = lax.rem(me + o, n)
        ref = w1s.at[src, at_rows(dp * half, half)]
        return pltpu.make_async_remote_copy(
            src_ref=ref, dst_ref=ref, send_sem=w1_send.at[src], recv_sem=w1_recv.at[src],
            device_id={"ra": src})

    def dp_copy(o, p):
        src = lax.rem(me + o, n)
        ref = w1s.at[src, at_rows(dp * half, half)]
        return pltpu.make_async_remote_copy(
            src_ref=ref, dst_ref=ref, send_sem=dp_send.at[src, p], recv_sem=dp_recv.at[src, dp],
            device_id={"dp": lax.rem(dp + p, nd)})

    def dp_landed(o, p):
        src = lax.rem(me + o, n)
        sender = lax.rem(dp + p, nd)
        ref = w1s.at[src, at_rows(sender * half, half)]
        return pltpu.make_async_remote_copy(
            src_ref=ref, dst_ref=ref, send_sem=dp_send.at[src, p], recv_sem=dp_recv.at[src, sender],
            device_id={"dp": sender})

    start_own(make_x)
    for o in range(1, n):
        w1_copy(o).start()

    def x_landed(src):
        for o in range(1, m):
            xy_copy(src, o).start()

    relay(make_x, x_landed)
    for o in range(1, n):
        w1_landed(o).wait_recv()
        for p in range(1, nd):
            dp_copy(o, p).start()
    own_w1.wait()
    own_w2.wait()
    for o in range(1, n):
        for q in range(1, m):
            xy_landed(lax.rem(me + o, n), q).wait_recv()
        for p in range(1, nd):
            dp_landed(o, p).wait_recv()

    def make_h(b):
        return functools.partial(
            line, lambda s: h.at[s, at_rows(b * block, block)],
            lambda s: h_r.at[b, s], lambda s: h_l.at[b, s], lambda s: h_recv.at[b, s])

    def rs_copy(b, o):
        to = lax.rem(cb + o, m)
        return pltpu.make_async_remote_copy(
            src_ref=rs_src.at[b, at_rows(to * rows, rows)], dst_ref=rs_recv.at[b, cb],
            send_sem=rs_send.at[b, o], recv_sem=rs_rcv.at[b, cb], device_id={"cb": to})

    def rs_landed(b, o):
        sender = lax.rem(cb + o, m)
        ref = rs_recv.at[b, sender]
        return pltpu.make_async_remote_copy(
            src_ref=ref, dst_ref=ref, send_sem=rs_send.at[b, o], recv_sem=rs_rcv.at[b, sender],
            device_id={"cb": sender})

    def st_copy(b, o):
        return pltpu.make_async_remote_copy(
            src_ref=st_src.at[b], dst_ref=st_recv.at[b, me],
            send_sem=st_send.at[b, o], recv_sem=st_rcv.at[b, me],
            device_id={"ra": lax.rem(me + o, n)})

    def st_landed(b, o):
        sender = lax.rem(me + o, n)
        ref = st_recv.at[b, sender]
        return pltpu.make_async_remote_copy(
            src_ref=ref, dst_ref=ref, send_sem=st_send.at[b, o], recv_sem=st_rcv.at[b, sender],
            device_id={"ra": sender})

    def fin_copy(b, o):
        ref = fin.at[at_rows(b * block + cb * rows, rows)]
        return pltpu.make_async_remote_copy(
            src_ref=ref, dst_ref=ref, send_sem=fin_send.at[b, o], recv_sem=fin_rcv.at[b, cb],
            device_id={"cb": lax.rem(cb + o, m)})

    def fin_landed(b, o):
        sender = lax.rem(cb + o, m)
        ref = fin.at[at_rows(b * block + sender * rows, rows)]
        return pltpu.make_async_remote_copy(
            src_ref=ref, dst_ref=ref, send_sem=fin_send.at[b, o], recv_sem=fin_rcv.at[b, sender],
            device_id={"cb": sender})

    def up(b):
        here = at_rows(b * block, block)

        @pl.loop(0, fs // tile)
        def _(t):
            cols = at_rows(t * tile, tile)
            acc = jnp.dot(xall[0, here, :], w1s[0, :, cols], preferred_element_type=jnp.float32)
            for k in range(1, n):
                acc += jnp.dot(xall[k, here, :], w1s[k, :, cols], preferred_element_type=jnp.float32)
            h[me, here, cols] = jnp.square(jnp.maximum(acc, 0.0)).astype(jnp.bfloat16)
        start_own(make_h(b))

    def down(b):
        here = at_rows(b * block, block)
        relay(make_h(b), lambda src: None)

        @pl.loop(0, dl // tile)
        def _(t):
            cols = at_rows(t * tile, tile)
            acc = jnp.dot(h[0, here, :], w2[pl.ds(0, fs), cols], preferred_element_type=jnp.float32)
            for k in range(1, n):
                acc += jnp.dot(h[k, here, :], w2[pl.ds(k * fs, fs), cols],
                               preferred_element_type=jnp.float32)
            part[:, cols] = acc
            rs_src[b, :, cols] = acc.astype(jnp.bfloat16)
        for o in range(1, m):
            rs_copy(b, o).start()
        mixed[b] = part[at_rows(cb * rows, rows), :] + residual_scale * xall[
            me, at_rows(b * block + cb * rows, rows), :].astype(jnp.float32)

    def reduce(b):
        total = mixed[b]
        for o in range(1, m):
            rs_landed(b, o).wait_recv()
            total += rs_recv[b, lax.rem(cb + o, m)].astype(jnp.float32)
        mixed[b] = total
        lane = lax.broadcasted_iota(jnp.int32, (rows, 128), 1)
        st_src[b] = jnp.where(
            lane < 64, jnp.sum(total, axis=1, keepdims=True),
            jnp.sum(total * total, axis=1, keepdims=True))
        for o in range(1, n):
            st_copy(b, o).start()

    def finish(b):
        sums = st_src[b]
        for o in range(1, n):
            st_landed(b, o).wait_recv()
            sums += st_recv[b, lax.rem(me + o, n)]
        mean = sums[:, 0:1] / width
        spread = sums[:, 64:65] / width - mean * mean
        fin[at_rows(b * block + cb * rows, rows), :] = (
            (mixed[b] - mean) * lax.rsqrt(spread + norm_eps) * gain_ref[...] + bias_ref[...]
        ).astype(jnp.bfloat16)
        for o in range(1, m):
            fin_copy(b, o).start()

    @pl.loop(0, blocks + lookahead + 2)
    def _(step):
        for lag, stage in ((0, up), (lookahead, down), (lookahead + 1, reduce),
                           (lookahead + 2, finish)):
            @pl.when((step >= lag) & (step < blocks + lag))
            def _():
                stage(step - lag)

    @pl.loop(0, blocks)
    def _(b):
        for o in range(1, m):
            fin_landed(b, o).wait_recv()
    out = pltpu.make_async_copy(fin, o_hbm, loc_sem.at[3])
    out.start()
    line_sent(make_x)
    for o in range(1, n):
        w1_copy(o).wait_send()
        for q in range(1, m):
            xy_copy(lax.rem(me + o, n), q).wait_send()
        for p in range(1, nd):
            dp_copy(o, p).wait_send()

    @pl.loop(0, blocks)
    def _(b):
        line_sent(make_h(b))
        for o in range(1, m):
            rs_copy(b, o).wait_send()
            fin_copy(b, o).wait_send()
        for o in range(1, n):
            st_copy(b, o).wait_send()
    out.wait()


def feed_forward(normed, up_weight, down_weight, gain_out, bias_out):
    n, m, nd = lax.axis_size("ra"), lax.axis_size("cb"), lax.axis_size("dp")
    tokens, dl = normed.shape
    fl = up_weight.shape[1]
    fs = fl // n
    block = math.gcd(tokens, 256)
    blocks = tokens // block
    rows = block // m
    dma = pltpu.SemaphoreType.DMA
    bf16, f32 = jnp.bfloat16, jnp.float32
    hbm = pl.BlockSpec(memory_space=pl.ANY)
    vmem = pl.BlockSpec(memory_space=pltpu.VMEM)
    return pl.pallas_call(
        functools.partial(kernel, n, m, nd, block),
        out_shape=jax.ShapeDtypeStruct((tokens, dl), bf16),
        in_specs=[hbm, hbm, hbm, vmem, vmem],
        out_specs=hbm,
        scratch_shapes=[
            pltpu.VMEM((n, tokens, dl), bf16),
            pltpu.VMEM((n, dl, fs), bf16),
            pltpu.VMEM((n, tokens, fs), bf16),
            pltpu.VMEM((fl, dl), bf16),
            pltpu.VMEM((block, dl), f32),
            pltpu.VMEM((blocks, block, dl), bf16),
            pltpu.VMEM((blocks, m, rows, dl), bf16),
            pltpu.VMEM((blocks, rows, dl), f32),
            pltpu.VMEM((blocks, rows, 128), f32),
            pltpu.VMEM((blocks, n, rows, 128), f32),
            pltpu.VMEM((tokens, dl), bf16),
            dma((4,)), dma((n,)), dma((n,)), dma((n, nd)), dma((n, nd)),
            dma((n,)), dma((n,)), dma((n,)), dma((n, m)), dma((n, m)),
            dma((blocks, n)), dma((blocks, n)), dma((blocks, n)),
            dma((blocks, m)), dma((blocks, m)), dma((blocks, n)), dma((blocks, n)),
            dma((blocks, m)), dma((blocks, m)),
        ],
        compiler_params=pltpu.CompilerParams(
            collective_id=0, has_side_effects=True, vmem_limit_bytes=66 * 1000 * 1000),
    )(normed, up_weight, down_weight, gain_out.reshape(1, dl), bias_out.reshape(1, dl))


def per_device(carried, branch_in, gain_in, bias_in, up_weight, down_weight, gain_out, bias_out):
    width = carried.shape[1] * lax.axis_size("ra")
    mixed_in = residual_scale * carried.astype(jnp.float32) + branch_in.astype(jnp.float32)
    totals, squares = lax.psum(
        (jnp.sum(mixed_in, axis=1), jnp.sum(mixed_in * mixed_in, axis=1)), "ra"
    )
    mean = totals[:, None] / width
    spread = squares[:, None] / width - mean * mean
    normed = ((mixed_in - mean) * lax.rsqrt(spread + norm_eps) * gain_in + bias_in).astype(
        jnp.bfloat16)
    return feed_forward(normed, up_weight, down_weight, gain_out, bias_out)


def solution(mesh):
    in_specs = (
        P("dp", "ra"),
        P("dp", "ra"),
        P("ra"),
        P("ra"),
        P("ra", "cb"),
        P("cb", "ra"),
        P("ra"),
        P("ra"),
    )
    out_specs = P("dp", "ra")
    return jax.shard_map(
        per_device, mesh=mesh, in_specs=in_specs, out_specs=out_specs, check_vma=False
    )
```

time: 860 us -> 436 us (0.51)
  Pallas kernels: 0 us -> 401 us
  blocking collectives: 412 us -> 20.5 us
  waiting for transfers between devices: 353 us -> 0 us
  matrix products: 38.6 us -> 0 us
  local copies, waits for them, and re-layouts: 23.6 us -> 3.87 us
  between operations: 13.2 us -> 0.04 us
  other arithmetic: 18.1 us -> 9.05 us
    pallas_call x0 -> x1, Pallas kernels: none -> 401 us  [feed_forward(): pl.pallas_call(functools.partial(kernel, n, m, nd, block), out_shape=jax....]
    all_to_all x1 -> x0, blocking collectives: 373 us -> none  [per_device(): lax.all_to_all(up_weight, 'ra', split_axis=1, concat_axis=0, tiled=True)]
    all_gather x2 -> x0, waiting for transfers between devices: 217 us -> none  [the longest x1 217 us: per_device(): lax.all_gather(hidden_share, 'ra', axis=0, tiled=True)]
    psum x1 -> x0, waiting for transfers between devices: 136 us -> none  [per_device(): branch_out = lax.psum(branch_part, 'cb')]
    dot_general x2 -> x0, matrix products: 38.6 us -> none  [the longest x1 19.5 us: per_device(): lax.dot_general(lax.all_gather(hidden_share, 'ra', axis=0, tiled=True), d...]
    psum x1 -> x0, blocking collectives: 18.7 us -> none  [per_device(): lax.psum((jnp.sum(mixed_out, axis=1), jnp.sum(mixed_out * mixed_out, axis...]
    all_to_all x1 -> x0, local copies, waits for them, and re-layouts: 11.4 us -> none  [per_device(): lax.all_to_all(up_weight, 'ra', split_axis=1, concat_axis=0, tiled=True)]
  transfers between devices with their start and end apart: 3 -> 0, of which waited for: 2 -> 0; matrix products, arithmetic and copies ran while one was open for 3% -> 0% of each run, Pallas kernels for 0% -> 0%
where the time goes in v1:
time: 436 us; the launch traced here: 434 us
  Pallas kernels  401 us (92%)
  blocking collectives  20.5 us (5%)
  other arithmetic  9.05 us (2%)
    pallas_call x1, Pallas kernels, feed_forward(): pl.pallas_call(functools.partial(kernel, n, m, nd, block), out_shape=jax....  401 us
    psum x1, blocking collectives, per_device(): lax.psum((jnp.sum(mixed_in, axis=1), jnp.sum(mixed_in * mixed_in, axis=1)...  20.5 us

profile of v1, /device:TPU:0, one launch (start us, length us, event | category | flops | bytes accessed | tf_op | source)
XLA Modules:
  0.0 434.2 jit_solution(10267801099152904327)
XLA Ops:
  0.0 0.0 copy-start
  0.0 0.0 copy-start.1
  0.0 0.0 copy-start.2
  0.0 4.5 %fusion = (f32[1536]{0:T(1024)S(1)}, f32[1536]{0:T(1024)S(1)}) fusion(bf16[1536,1024]{1,0:T(8,128)(2,1)} %param.9, bf16[1536,1024]{1,0:T(8,128)(2,1)} %param.8), kind=kLoop, calls=%fused_computation.3 | loop fusion | flops 11006976 | bytes 6303744 | tf_op jit(solution)/shard_map/reduce_sum | solution.py:343
  4.5 20.5 %all-reduce = (f32[1536]{0:T(1024)S(1)}, f32[1536]{0:T(1024)S(1)}) all-reduce(f32[1536]{0:T(1024)S(1)} %get-tuple-element.6, f32[1536]{0:T(1024)S(1)} %get-tuple-element.5), channel_id=1, replica_groups=mesh['ra'=4,'cb'=4,'dp'=2] {'ra'}, use_global_device_ids=true, to_apply=%region_3.0 | all-reduce | flops 3072 | bytes 24576 | tf_op jit(solution)/shard_map/psum | solution.py:342
  25.1 0.0 copy-done
  25.1 0.0 copy-done.1
  25.1 0.0 copy-done.2
  25.1 4.5 %add_convert_fusion.x_hbm = bf16[1536,1024]{1,0:T(8,128)(2,1)} fusion(bf16[1536,1024]{1,0:T(8,128)(2,1)S(1)} %copy-done, bf16[1536,1024]{1,0:T(8,128)(2,1)} %param.8, f32[1024]{0:T(1024)S(1)} %copy-done.1, f32[1024]{0:T(1024)S(1)} %copy-done.2, f32[1536]{0:T(1024)S(1)} %get-tuple-element.10, f32[1536]{0:T(1024)S(1)} %get-tuple-element.9), kind=kLoop, calls=%fused_computation | loop fusion | flops 14155776 | bytes 9457664 | tf_op jit(solution)/shard_map/convert_element_type | solution.py:347
  29.6 400.7 %shard_map.82 = bf16[1536,1024]{1,0:T(8,128)(2,1)} custom-call(bf16[1536,1024]{1,0:T(8,128)(2,1)} %add_convert_fusion.x_hbm, bf16[1024,4096]{1,0:T(8,128)(2,1)} %w1_hbm.1, bf16[4096,1024]{1,0:T(8,128)(2,1)} %w2_hbm.1, f32[1,1024]{1,0:T(1,128)} %bitcast.2, f32[1,1024]{1,0:T(1,128)} %bitcast.3), custom_call_target="tpu_custom_call" | custom-call | tf_op jit(solution)/shard_map/pallas_call | solution.py:311
  430.3 3.9 copy.10
  (1 shorter events, 0.0 us)
Async XLA Ops:
  0.0 25.1 %copy-start = (bf16[1536,1024]{1,0:T(8,128)(2,1)S(1)}, bf16[1536,1024]{1,0:T(8,128)(2,1)}, u32[]{:S(2)}) copy-start(bf16[1536,1024]{1,0:T(8,128)(2,1)} %param.9) | copy-start | bytes 9437188
  0.0 25.1 %copy-start.1 = (f32[1024]{0:T(1024)S(1)}, f32[1024]{0:T(1024)}, u32[]{:S(2)}) copy-start(f32[1024]{0:T(1024)} %param.11) | copy-start | bytes 12292
  0.0 25.1 %copy-start.2 = (f32[1024]{0:T(1024)S(1)}, f32[1024]{0:T(1024)}, u32[]{:S(2)}) copy-start(f32[1024]{0:T(1024)} %param.10) | copy-start | bytes 12292

commit v2 on v1

--- a/solution.py
+++ b/solution.py
@@ -13,8 +13,8 @@
 lookahead = 2
 
 
-def kernel(n, m, nd, block, x_hbm, w1_hbm, w2_hbm, gain_ref, bias_ref, o_hbm,
-           xall, w1s, h, w2, part, rs_src, rs_recv, mixed, st_src, st_recv, fin,
+def kernel(n, m, nd, block, carried_hbm, branch_hbm, w1_hbm, w2_hbm, gain_in_ref, bias_in_ref,
+           gain_ref, bias_ref, o_hbm, s1_src, s1_recv, s1_tot, s1_send, s1_rcv, xall, w1s, h, w2, part, rs_src, rs_recv, mixed, st_src, st_recv, fin,
            loc_sem, w1_send, w1_recv, dp_send, dp_recv, xz_r, xz_l, xz_recv,
            xy_send, xy_recv, h_r, h_l, h_recv, rs_send, rs_rcv, st_send, st_rcv,
            fin_send, fin_rcv):
@@ -25,6 +25,8 @@
     quarter = tokens // m
     rows = block // m
     half = dl // nd
+    pieces = w1_send.shape[1]
+    piece = half // pieces
     width = n * dl
     tile = math.gcd(256, math.gcd(fs, dl))
 
@@ -36,15 +38,16 @@
     for o in range(1, nd):
         pl.semaphore_signal(barrier, inc=1, device_id={"dp": lax.rem(dp + o, nd)})
 
-    own_x = pltpu.make_async_copy(x_hbm, xall.at[me], loc_sem.at[0])
+    own_carried = pltpu.make_async_copy(carried_hbm, fin, loc_sem.at[0])
+    own_branch = pltpu.make_async_copy(branch_hbm, rs_src, loc_sem.at[4])
     own_w1 = pltpu.make_async_copy(
         w1_hbm.at[:, pl.ds(pl.multiple_of(me * fs, fs), fs)], w1s.at[me], loc_sem.at[1])
     own_w2 = pltpu.make_async_copy(w2_hbm, w2, loc_sem.at[2])
-    own_x.start()
+    own_carried.start()
+    own_branch.start()
     own_w1.start()
     own_w2.start()
     pl.semaphore_wait(barrier, n + m + nd - 3)
-    own_x.wait()
 
     def at_rows(start, size):
         return pl.ds(pl.multiple_of(start, size), size)
@@ -66,7 +69,7 @@
         def _():
             make(me, False).start()
 
-    def relay(make, landed):
+    def relay(make, landed, between=None):
         for s in range(1, n):
             @pl.when(me - s >= 0)
             def _():
@@ -85,6 +88,8 @@
                 def _():
                     make(me + s, False).start()
                 landed(me + s)
+            if between is not None:
+                between(s)
 
     def line_sent(make):
         for s in range(n):
@@ -113,19 +118,55 @@
             src_ref=ref, dst_ref=ref, send_sem=xy_send.at[src, o], recv_sem=xy_recv.at[src, sender],
             device_id={"cb": sender})
 
-    def w1_copy(o):
+    def w1_copy(o, p):
         to = lax.rem(me + o, n)
-        return pltpu.make_async_remote_copy(
-            src_ref=w1_hbm.at[at_rows(dp * half, half), pl.ds(pl.multiple_of(to * fs, fs), fs)],
-            dst_ref=w1s.at[me, at_rows(dp * half, half)],
-            send_sem=w1_send.at[to], recv_sem=w1_recv.at[me], device_id={"ra": to})
-
-    def w1_landed(o):
+        here = at_rows(dp * half + p * piece, piece)
+        return pltpu.make_async_remote_copy(
+            src_ref=w1_hbm.at[here, pl.ds(pl.multiple_of(to * fs, fs), fs)],
+            dst_ref=w1s.at[me, here],
+            send_sem=w1_send.at[to, p], recv_sem=w1_recv.at[me, p], device_id={"ra": to})
+
+    def w1_landed(o, p):
         src = lax.rem(me + o, n)
-        ref = w1s.at[src, at_rows(dp * half, half)]
-        return pltpu.make_async_remote_copy(
-            src_ref=ref, dst_ref=ref, send_sem=w1_send.at[src], recv_sem=w1_recv.at[src],
+        ref = w1s.at[src, at_rows(dp * half + p * piece, piece)]
+        return pltpu.make_async_remote_copy(
+            src_ref=ref, dst_ref=ref, send_sem=w1_send.at[src, p], recv_sem=w1_recv.at[src, p],
             device_id={"ra": src})
+
+    def w1_pieces(p):
+        if p < pieces:
+            for o in range(1, n):
+                w1_copy(o, p).start()
+
+    def s1_copy(o):
+        return pltpu.make_async_remote_copy(
+            src_ref=s1_src, dst_ref=s1_recv.at[me], send_sem=s1_send.at[o],
+            recv_sem=s1_rcv.at[me], device_id={"ra": lax.rem(me + o, n)})
+
+    def s1_landed(o):
+        sender = lax.rem(me + o, n)
+        ref = s1_recv.at[sender]
+        return pltpu.make_async_remote_copy(
+            src_ref=ref, dst_ref=ref, send_sem=s1_send.at[o], recv_sem=s1_rcv.at[sender],
+            device_id={"ra": sender})
+
+    chunks = tokens // 128
+
+    def mixed_in(here):
+        return residual_scale * fin[here, :].astype(jnp.float32) + rs_src[here, :].astype(
+            jnp.float32)
+
+    def sums_of(total):
+        lane = lax.broadcasted_iota(jnp.int32, (total.shape[0], 128), 1)
+        tile = jnp.where(
+            lane < 64, jnp.sum(total, axis=1, keepdims=True),
+            jnp.sum(total * total, axis=1, keepdims=True))
+        if total.shape[0] < 128:
+            tile = jnp.concatenate([tile] * (128 // total.shape[0]), axis=0)
+        return tile.T
+
+    def column(row):
+        return jnp.broadcast_to(row, (128, 128)).T[:, 0:1]
 
     def dp_copy(o, p):
         src = lax.rem(me + o, n)
@@ -142,17 +183,44 @@
             src_ref=ref, dst_ref=ref, send_sem=dp_send.at[src, p], recv_sem=dp_recv.at[src, sender],
             device_id={"dp": sender})
 
+    w1_pieces(0)
+    own_carried.wait()
+    own_branch.wait()
+
+    @pl.loop(0, chunks)
+    def _(c):
+        sums = sums_of(mixed_in(at_rows(c * 128, 128)))
+        s1_src[pl.ds(c, 1), :] = sums[0:1, :]
+        s1_src[pl.ds(chunks + c, 1), :] = sums[64:65, :]
+    for o in range(1, n):
+        s1_copy(o).start()
+    s1_tot[...] = s1_src[...]
+    for o in range(1, n):
+        s1_landed(o).wait_recv()
+        s1_tot[...] += s1_recv[lax.rem(me + o, n)]
+
+    @pl.loop(0, chunks)
+    def _(c):
+        here = at_rows(c * 128, 128)
+        mean_row = s1_tot[pl.ds(c, 1), :] / width
+        scale_row = lax.rsqrt(s1_tot[pl.ds(chunks + c, 1), :] / width - mean_row * mean_row + norm_eps)
+        xall[me, here, :] = (
+            (mixed_in(here) - column(mean_row)) * column(scale_row) * gain_in_ref[...]
+            + bias_in_ref[...]
+        ).astype(jnp.bfloat16)
     start_own(make_x)
-    for o in range(1, n):
-        w1_copy(o).start()
+    w1_pieces(1)
 
     def x_landed(src):
         for o in range(1, m):
             xy_copy(src, o).start()
 
-    relay(make_x, x_landed)
-    for o in range(1, n):
-        w1_landed(o).wait_recv()
+    relay(make_x, x_landed, lambda s: w1_pieces(s + 1))
+    for p in range(n + 1, pieces):
+        w1_pieces(p)
+    for o in range(1, n):
+        for p in range(pieces):
+            w1_landed(o, p).wait_recv()
         for p in range(1, nd):
             dp_copy(o, p).start()
     own_w1.wait()
@@ -171,7 +239,7 @@
     def rs_copy(b, o):
         to = lax.rem(cb + o, m)
         return pltpu.make_async_remote_copy(
-            src_ref=rs_src.at[b, at_rows(to * rows, rows)], dst_ref=rs_recv.at[b, cb],
+            src_ref=rs_src.at[at_rows(b * block + to * rows, rows)], dst_ref=rs_recv.at[b, cb],
             send_sem=rs_send.at[b, o], recv_sem=rs_rcv.at[b, cb], device_id={"cb": to})
 
     def rs_landed(b, o):
@@ -231,7 +299,7 @@
                 acc += jnp.dot(h[k, here, :], w2[pl.ds(k * fs, fs), cols],
                                preferred_element_type=jnp.float32)
             part[:, cols] = acc
-            rs_src[b, :, cols] = acc.astype(jnp.bfloat16)
+            rs_src[here, cols] = acc.astype(jnp.bfloat16)
         for o in range(1, m):
             rs_copy(b, o).start()
         mixed[b] = part[at_rows(cb * rows, rows), :] + residual_scale * xall[
@@ -243,10 +311,8 @@
             rs_landed(b, o).wait_recv()
             total += rs_recv[b, lax.rem(cb + o, m)].astype(jnp.float32)
         mixed[b] = total
-        lane = lax.broadcasted_iota(jnp.int32, (rows, 128), 1)
-        st_src[b] = jnp.where(
-            lane < 64, jnp.sum(total, axis=1, keepdims=True),
-            jnp.sum(total * total, axis=1, keepdims=True))
+        sums = sums_of(total)
+        st_src[b] = jnp.concatenate([sums[0:4, :], sums[64:68, :]], axis=0)
         for o in range(1, n):
             st_copy(b, o).start()
 
@@ -255,10 +321,11 @@
         for o in range(1, n):
             st_landed(b, o).wait_recv()
             sums += st_recv[b, lax.rem(me + o, n)]
-        mean = sums[:, 0:1] / width
-        spread = sums[:, 64:65] / width - mean * mean
+        mean_row = sums[0:1, :] / width
+        scale_row = lax.rsqrt(sums[4:5, :] / width - mean_row * mean_row + norm_eps)
+        mean, scale = column(mean_row)[0:rows], column(scale_row)[0:rows]
         fin[at_rows(b * block + cb * rows, rows), :] = (
-            (mixed[b] - mean) * lax.rsqrt(spread + norm_eps) * gain_ref[...] + bias_ref[...]
+            (mixed[b] - mean) * scale * gain_ref[...] + bias_ref[...]
         ).astype(jnp.bfloat16)
         for o in range(1, m):
             fin_copy(b, o).start()
@@ -279,7 +346,9 @@
     out.start()
     line_sent(make_x)
     for o in range(1, n):
-        w1_copy(o).wait_send()
+        s1_copy(o).wait_send()
+        for p in range(pieces):
+            w1_copy(o, p).wait_send()
         for q in range(1, m):
             xy_copy(lax.rem(me + o, n), q).wait_send()
         for p in range(1, nd):
@@ -296,14 +365,16 @@
     out.wait()
 
 
-def feed_forward(normed, up_weight, down_weight, gain_out, bias_out):
+def per_device(carried, branch_in, gain_in, bias_in, up_weight, down_weight, gain_out, bias_out):
     n, m, nd = lax.axis_size("ra"), lax.axis_size("cb"), lax.axis_size("dp")
-    tokens, dl = normed.shape
+    tokens, dl = carried.shape
     fl = up_weight.shape[1]
     fs = fl // n
     block = math.gcd(tokens, 256)
     blocks = tokens // block
     rows = block // m
+    pieces = 4
+    chunk_rows = -(-2 * (tokens // 128) // 8) * 8
     dma = pltpu.SemaphoreType.DMA
     bf16, f32 = jnp.bfloat16, jnp.float32
     hbm = pl.BlockSpec(memory_space=pl.ANY)
@@ -311,21 +382,25 @@
     return pl.pallas_call(
         functools.partial(kernel, n, m, nd, block),
         out_shape=jax.ShapeDtypeStruct((tokens, dl), bf16),
-        in_specs=[hbm, hbm, hbm, vmem, vmem],
+        in_specs=[hbm, hbm, hbm, hbm, vmem, vmem, vmem, vmem],
         out_specs=hbm,
         scratch_shapes=[
+            pltpu.VMEM((chunk_rows, 128), f32),
+            pltpu.VMEM((n, chunk_rows, 128), f32),
+            pltpu.VMEM((chunk_rows, 128), f32),
+            dma((n,)), dma((n,)),
             pltpu.VMEM((n, tokens, dl), bf16),
             pltpu.VMEM((n, dl, fs), bf16),
             pltpu.VMEM((n, tokens, fs), bf16),
             pltpu.VMEM((fl, dl), bf16),
             pltpu.VMEM((block, dl), f32),
-            pltpu.VMEM((blocks, block, dl), bf16),
+            pltpu.VMEM((tokens, dl), bf16),
             pltpu.VMEM((blocks, m, rows, dl), bf16),
             pltpu.VMEM((blocks, rows, dl), f32),
-            pltpu.VMEM((blocks, rows, 128), f32),
-            pltpu.VMEM((blocks, n, rows, 128), f32),
+            pltpu.VMEM((blocks, 8, 128), f32),
+            pltpu.VMEM((blocks, n, 8, 128), f32),
             pltpu.VMEM((tokens, dl), bf16),
-            dma((4,)), dma((n,)), dma((n,)), dma((n, nd)), dma((n, nd)),
+            dma((5,)), dma((n, pieces)), dma((n, pieces)), dma((n, nd)), dma((n, nd)),
             dma((n,)), dma((n,)), dma((n,)), dma((n, m)), dma((n, m)),
             dma((blocks, n)), dma((blocks, n)), dma((blocks, n)),
             dma((blocks, m)), dma((blocks, m)), dma((blocks, n)), dma((blocks, n)),
@@ -333,20 +408,8 @@
         ],
         compiler_params=pltpu.CompilerParams(
             collective_id=0, has_side_effects=True, vmem_limit_bytes=66 * 1000 * 1000),
-    )(normed, up_weight, down_weight, gain_out.reshape(1, dl), bias_out.reshape(1, dl))
-
-
-def per_device(carried, branch_in, gain_in, bias_in, up_weight, down_weight, gain_out, bias_out):
-    width = carried.shape[1] * lax.axis_size("ra")
-    mixed_in = residual_scale * carried.astype(jnp.float32) + branch_in.astype(jnp.float32)
-    totals, squares = lax.psum(
-        (jnp.sum(mixed_in, axis=1), jnp.sum(mixed_in * mixed_in, axis=1)), "ra"
-    )
-    mean = totals[:, None] / width
-    spread = squares[:, None] / width - mean * mean
-    normed = ((mixed_in - mean) * lax.rsqrt(spread + norm_eps) * gain_in + bias_in).astype(
-        jnp.bfloat16)
-    return feed_forward(normed, up_weight, down_weight, gain_out, bias_out)
+    )(carried, branch_in, up_weight, down_weight, gain_in.reshape(1, dl), bias_in.reshape(1, dl),
+      gain_out.reshape(1, dl), bias_out.reshape(1, dl))
 
 
 def solution(mesh):

time: 436 us -> 392 us (0.90)
  blocking collectives: 20.5 us -> 0 us
  Pallas kernels: 401 us -> 388 us
  other arithmetic: 9.05 us -> 0 us
    psum x1 -> x0, blocking collectives: 20.5 us -> none  [per_device(): lax.psum((jnp.sum(mixed_in, axis=1), jnp.sum(mixed_in * mixed_in, axis=1)...]
    pallas_call x1, Pallas kernels: 401 us -> 388 us  [per_device(): pl.pallas_call(functools.partial(kernel, n, m, nd, block), out_shape=jax....]
    convert_element_type x1 -> x0, other arithmetic: 4.53 us -> none  [per_device(): ((mixed_in - mean) * lax.rsqrt(spread + norm_eps) * gain_in + bias_in).as...]
    reduce_sum x1 -> x0, other arithmetic: 4.51 us -> none  [per_device(): jnp.sum(mixed_in, axis=1)]
where the time goes in v2:
time: 392 us
  Pallas kernels  388 us (99%)
    pallas_call x1, Pallas kernels, per_device(): pl.pallas_call(functools.partial(kernel, n, m, nd, block), out_shape=jax....  388 us

profile of v2, /device:TPU:0, one launch (start us, length us, event | category | flops | bytes accessed | tf_op | source)
XLA Modules:
  0.0 391.6 jit_solution(3056178977891014765)
XLA Ops:
  0.0 387.7 %shard_map.82 = bf16[1536,1024]{1,0:T(8,128)(2,1)} custom-call(bf16[1536,1024]{1,0:T(8,128)(2,1)} %carried_hbm.1, bf16[1536,1024]{1,0:T(8,128)(2,1)} %branch_hbm.1, bf16[1024,4096]{1,0:T(8,128)(2,1)} %w1_hbm.1, bf16[4096,1024]{1,0:T(8,128)(2,1)} %w2_hbm.1, f32[1,1024]{1,0:T(1,128)} %bitcast.4, f32[1,1024]{1,0:T(1,128)} %bitcast.5, f32[1,1024]{1,0:T(1,128)} %bitcast.6, ...), custom_call_target="tpu_custom_call" | custom-call | tf_op jit(solution)/shard_map/pallas_call | solution.py:382
  387.7 3.9 copy.10

commit v3 on v2

--- a/solution.py
+++ b/solution.py
@@ -10,7 +10,7 @@
 
 residual_scale = 2.0**0.25
 norm_eps = 1e-05
-lookahead = 2
+lookahead = 4
 
 
 def kernel(n, m, nd, block, carried_hbm, branch_hbm, w1_hbm, w2_hbm, gain_in_ref, bias_in_ref,
@@ -370,7 +370,7 @@
     tokens, dl = carried.shape
     fl = up_weight.shape[1]
     fs = fl // n
-    block = math.gcd(tokens, 256)
+    block = math.gcd(tokens, 128)
     blocks = tokens // block
     rows = block // m
     pieces = 4

time: 392 us -> 388 us (0.990)
  Pallas kernels: 388 us -> 384 us
where the time goes in v3:
time: 388 us
  Pallas kernels  384 us (99%)
    pallas_call x1, Pallas kernels, per_device(): pl.pallas_call(functools.partial(kernel, n, m, nd, block), out_shape=jax....  384 us

profile of v3, /device:TPU:0, one launch (start us, length us, event | category | flops | bytes accessed | tf_op | source)
XLA Modules:
  0.0 387.8 jit_solution(10451540366887437405)
XLA Ops:
  0.0 384.0 %shard_map.82 = bf16[1536,1024]{1,0:T(8,128)(2,1)} custom-call(bf16[1536,1024]{1,0:T(8,128)(2,1)} %carried_hbm.1, bf16[1536,1024]{1,0:T(8,128)(2,1)} %branch_hbm.1, bf16[1024,4096]{1,0:T(8,128)(2,1)} %w1_hbm.1, bf16[4096,1024]{1,0:T(8,128)(2,1)} %w2_hbm.1, f32[1,1024]{1,0:T(1,128)} %bitcast.4, f32[1,1024]{1,0:T(1,128)} %bitcast.5, f32[1,1024]{1,0:T(1,128)} %bitcast.6, ...), custom_call_target="tpu_custom_call" | custom-call | tf_op jit(solution)/shard_map/pallas_call | solution.py:382
  384.0 3.9 copy.10
